TPU v7x, 256 devices: a whole 4x4x8 slice. The times are simulated.
256 devices in a mesh: sp: 32 (over z, x), tp: 8 (over y, core).
Axes of the slice: x: 4, y: 4, z: 8, core: 2. Of those that a mesh axis runs over, the one named last changes fastest.
Arguments:
- tokens: bfloat16 [16384, 2048], P(('sp', 'tp')), may hold values from -40 to 40
- query_weight: bfloat16 [2048, 1024], P(None, 'tp'), may hold values from -0.1875 to 0.1875
- key_weight: bfloat16 [2048, 256], replicated, may hold values from -0.1875 to 0.1875
- value_weight: bfloat16 [2048, 256], replicated, may hold values from -0.125 to 0.125
- out_weight: bfloat16 [1024, 2048], replicated, may hold values from -0.1875 to 0.1875
- head_gain: float32 [128], replicated, may hold values from 0.1 to 1.9
- lambdas: float32 [8], P('tp'), may hold values from 0.3 to 0.8
Outputs:
- mixed: bfloat16 [16384, 2048], P(('sp', 'tp'))
All inputs are finite; a program needn't handle non-finite values.
Results may differ from a plain program's by a relative error of at most 0.018.
The roundings to bfloat16 on the way count: a program that leaves them out, or rounds other values in their place, can miss the bound.
Values may be sent and summed in bfloat16 or wider, within the bound.
No kernel may reach another device: no remote copies, remote signals or barrier semaphores. Data moves between devices by JAX's collectives and lax.ppermute only.
A program may use at most 64 MiB of HBM per device.

v0:
```python
import jax
import jax.numpy as jnp
from jax import lax
from jax.sharding import PartitionSpec as P

H = 8
DH = 64
DV = 128
epsilon = 1e-06
rope_base = 10000.0
fold_span = 2048


def joined_along(parts, dim):
    parts = jnp.moveaxis(parts, 0, dim)
    shape = parts.shape
    return parts.reshape(*shape[:dim], shape[dim] * shape[dim + 1], *shape[dim + 2 :])


def copy_for_each(x, axis):
    count = lax.axis_size(axis)
    return lax.all_to_all(jnp.broadcast_to(x[None], (count, *x.shape)), axis, 0, 0, tiled=True)


def gather_directly(x, axis, dim):
    return joined_along(copy_for_each(x, axis), dim)


def sent_together(arrays, axis, dim, along):
    ends, at = ([], 0)
    for a in arrays[:-1]:
        at += a.shape[along]
        ends.append(at)
    both = jnp.concatenate(arrays, axis=along)
    return tuple(jnp.split(lax.all_gather(both, axis, axis=dim, tiled=True), ends, axis=along))


def rotate(tensor_in, places):
    head_dim = tensor_in.shape[-1]
    half_dim = head_dim // 2
    frequency = rope_base ** (-(jnp.arange(half_dim, dtype=jnp.float32) * 2.0) / head_dim)
    angles = places[:, None] * frequency[None, :]
    angles = angles.reshape((places.shape[0],) + (1,) * (tensor_in.ndim - 2) + (half_dim,))
    cosine = jnp.cos(angles)
    sine_part = jnp.sin(angles)
    first = tensor_in[..., :half_dim]
    second = tensor_in[..., half_dim:]
    return jnp.concatenate(
        [first * cosine - second * sine_part, first * sine_part + second * cosine], axis=-1
    )


def local(tokens, query_weight, key_weight, value_weight, out_weight, head_gain, lambdas):
    heads_dev = query_weight.shape[1] // (2 * DH)
    kv_heads = key_weight.shape[1] // (2 * DH)
    group_size = H // kv_heads
    kv_index = lax.axis_index("tp") * heads_dev // group_size
    key_cols = lax.dynamic_slice_in_dim(key_weight, kv_index * (2 * DH), 2 * DH, 1)
    value_cols = lax.dynamic_slice_in_dim(value_weight, kv_index * DV, DV, 1)
    stacked = jnp.concatenate([query_weight, key_cols, value_cols], axis=1)
    projected = jnp.dot(
        gather_directly(tokens, "tp", 0), stacked, preferred_element_type=jnp.float32
    )
    seq_rows = projected.shape[0]
    places = (lax.axis_index("sp") * seq_rows + jnp.arange(seq_rows, dtype=jnp.int32)).astype(
        jnp.float32
    )
    query_cols = heads_dev * 2 * DH
    queries = rotate(projected[:, :query_cols].reshape(seq_rows, heads_dev, 2, DH), places).astype(
        jnp.bfloat16
    )
    key_rows = rotate(
        projected[:, query_cols : query_cols + 2 * DH].reshape(seq_rows, 2, DH), places
    )
    key_rows = key_rows.astype(jnp.bfloat16).reshape(seq_rows, 2 * DH)
    value_rows = projected[:, query_cols + 2 * DH :].astype(jnp.bfloat16)
    score_scale = DH ** (-0.5)

    def update(carried, key_block, value_block):
        running_max, running_sum, weighted = carried
        scores = (
            jnp.einsum(
                "qhcd,kcd->cqhk",
                queries,
                key_block.reshape(key_block.shape[0], 2, DH),
                preferred_element_type=jnp.float32,
            )
            * score_scale
        )
        new_max = jnp.maximum(running_max, jnp.max(scores, axis=-1))
        weights = jnp.exp(scores - new_max[..., None])
        shrink = jnp.exp(running_max - new_max)
        running_sum = shrink * running_sum + jnp.sum(weights, axis=-1)
        weighted = shrink[..., None] * weighted + jnp.einsum(
            "cqhk,kv->cqhv",
            weights.astype(jnp.bfloat16),
            value_block,
            preferred_element_type=jnp.float32,
        )
        return (new_max, running_sum, weighted)

    initial = (
        jnp.full((2, seq_rows, heads_dev), -1e30, jnp.float32),
        jnp.zeros((2, seq_rows, heads_dev), jnp.float32),
        jnp.zeros((2, seq_rows, heads_dev, DV), jnp.float32),
    )
    key_piece, value_piece = sent_together((key_rows, value_rows), "sp", 0, 1)
    row_count = key_piece.shape[0]

    def one_span(state_now, span_index):
        key_block = lax.dynamic_slice_in_dim(key_piece, span_index * fold_span, fold_span, 0)
        value_block = lax.dynamic_slice_in_dim(value_piece, span_index * fold_span, fold_span, 0)
        return (update(state_now, key_block, value_block), None)

    running_max, running_sum, weighted = lax.scan(
        one_span, initial, jnp.arange(row_count // fold_span, dtype=jnp.int32)
    )[0]
    attended = (
        weighted[0] / running_sum[0][..., None]
        - lambdas[None, :, None] * weighted[1] / running_sum[1][..., None]
    )
    mean_square = jnp.mean(attended * attended, axis=-1, keepdims=True)
    normed = (attended * lax.rsqrt(mean_square + epsilon) * head_gain).astype(jnp.bfloat16)
    normed = normed.reshape(seq_rows, heads_dev * DV)
    regrouped = lax.all_to_all(normed, "tp", split_axis=0, concat_axis=1, tiled=True)
    return jnp.dot(regrouped, out_weight, preferred_element_type=jnp.float32).astype(jnp.bfloat16)


def solution(mesh):
    return jax.shard_map(
        local,
        mesh=mesh,
        in_specs=(P(("sp", "tp"), None), P(None, "tp"), P(), P(), P(), P(), P("tp")),
        out_specs=P(("sp", "tp"), None),
        check_vma=False,
    )
```

profile of v0, /device:TPU:1, one launch (start us, length us, event | category | flops | bytes accessed | tf_op | source)
XLA Modules:
  0.0 288.7 jit_solution(8956814849785031514)
XLA Ops:
  6.5 2.5 broadcast_in_dim.11
  9.1 6.7 %all-to-all-start = ((bf16[8,64,2048]{2,1,0:T(8,128)(2,1)}), bf16[8,64,2048]{2,1,0:T(8,128)(2,1)S(1)}, u32[]{:S(2)}, u32[]{:S(2)}) async-start(bf16[8,64,2048]{2,1,0:T(8,128)(2,1)} %broadcast_in_dim.11), calls=%async_computation | async-start | bytes 4194304 | tf_op jit(solution)/shard_map/all_to_all | solution.py:22
  17.4 24.6 %all-to-all-done = bf16[8,64,2048]{2,1,0:T(8,128)(2,1)S(1)} async-done(((bf16[8,64,2048]{2,1,0:T(8,128)(2,1)}), bf16[8,64,2048]{2,1,0:T(8,128)(2,1)S(1)}, u32[]{:S(2)}, u32[]{:S(2)}) %all-to-all-start) | async-done | bytes 2097184 | tf_op jit(solution)/shard_map/all_to_all | solution.py:22
  42.0 2.1 fusion.24
  45.7 98.9 %all-gather.2.cloned.1.call-done = bf16[16384,256]{0,1:T(8,128)(2,1)} async-done(((bf16[512,256]{0,1:T(8,128)(2,1)}), bf16[16384,256]{0,1:T(8,128)(2,1)}) %all-gather.2.cloned.1.call-update) | async-done | bytes 8388624 | tf_op jit(solution)/shard_map/all_gather | solution.py:35
  144.6 5.8 %fusion.33 = (bf16[16384,128]{0,1:T(8,128)(2,1)}, bf16[16384,128]{0,1:T(8,128)(2,1)}) fusion(bf16[16384,256]{0,1:T(8,128)(2,1)} %all-gather.2.cloned.1.call-done), kind=kLoop, calls=%fused_computation.57 | loop fusion | bytes 16777216 | tf_op jit(solution)/shard_map/split | solution.py:35
  150.4 113.6 %while.15 = (s32[]{:T(128)}, f32[2,512,1]{1,0,2:T(2,128)S(1)}, f32[2,512,1]{1,0,2:T(2,128)S(1)}, f32[2,512,1,128]{3,1,0,2:T(8,128)S(1)}, s32[8]{0:T(128)S(1)}, /...) while((s32[]{:T(128)}, f32[2,512,1]{1,0,2:T(2,128)S(1)}, ...), condition=%wide.region_3.4_spmd.clone, body=%wide.region_0.3_spmd.clone.sunk | while | flops 822482944 | bytes 62062812 | solution.py:115
  152.8 4.5 %bitcast_reduce_fusion.2 = (f32[2,512]{1,0:T(2,128)S(1)}, f32[2,2048,512]{2,1,0:T(8,128)}) fusion(bf16[2048,2,64]{0,2,1:T(8,128)(2,1)S(1)} %bitcast.99, bf16[512,1,2,64]{0,3,2,1:T(8,128)(2,1)S(1)} %get-tuple-element.234), kind=kOutput, calls=%fused_computation.1.clone.1 | convolution fusion | flops 272628736 | bytes 9048064 | tf_op jit(solution)/shard_map/while/body/eval_jaxpr/qhcd,kcd->cqhk/dot_general | solution.py:82
  157.3 5.3 %fusion.50 = f32[2,512,1,128]{3,1,0,2:T(8,128)S(1)} fusion(f32[2,2048,512]{2,1,0:T(8,128)} %get-tuple-element.202, f32[2,512]{1,0:T(2,128)S(1)} %bitcast.102, f32[2,512,1,128]{3,1,0,2:T(8,128)S(1)} %get-tuple-element.219, bf16[16384,128]{0,1:T(8,128)(2,1)} %get-tuple-element.235, s32[]{:T(128)S(6)} %select_n.17, ...), kind=kOutput, calls=%fused_computation.7.clone.1 | convolution fusion | flops 543555584 | bytes 9969669 | tf_op jit(solution)/shard_map/while/body/eval_jaxpr/cqhk,kv->cqhv/dot_general | solution.py:94
  163.2 1.4 fusion.49
  167.0 4.5 %bitcast_reduce_fusion.2 = (f32[2,512]{1,0:T(2,128)S(1)}, f32[2,2048,512]{2,1,0:T(8,128)}) fusion(bf16[2048,2,64]{0,2,1:T(8,128)(2,1)S(1)} %bitcast.99, bf16[512,1,2,64]{0,3,2,1:T(8,128)(2,1)S(1)} %get-tuple-element.234), kind=kOutput, calls=%fused_computation.1.clone.1 | convolution fusion | flops 272628736 | bytes 9048064 | tf_op jit(solution)/shard_map/while/body/eval_jaxpr/qhcd,kcd->cqhk/dot_general | solution.py:82
  171.5 5.3 %fusion.50 = f32[2,512,1,128]{3,1,0,2:T(8,128)S(1)} fusion(f32[2,2048,512]{2,1,0:T(8,128)} %get-tuple-element.202, f32[2,512]{1,0:T(2,128)S(1)} %bitcast.102, f32[2,512,1,128]{3,1,0,2:T(8,128)S(1)} %get-tuple-element.219, bf16[16384,128]{0,1:T(8,128)(2,1)} %get-tuple-element.235, s32[]{:T(128)S(6)} %select_n.17, ...), kind=kOutput, calls=%fused_computation.7.clone.1 | convolution fusion | flops 543555584 | bytes 9969669 | tf_op jit(solution)/shard_map/while/body/eval_jaxpr/cqhk,kv->cqhv/dot_general | solution.py:94
  177.4 1.4 fusion.49
  181.2 4.5 %bitcast_reduce_fusion.2 = (f32[2,512]{1,0:T(2,128)S(1)}, f32[2,2048,512]{2,1,0:T(8,128)}) fusion(bf16[2048,2,64]{0,2,1:T(8,128)(2,1)S(1)} %bitcast.99, bf16[512,1,2,64]{0,3,2,1:T(8,128)(2,1)S(1)} %get-tuple-element.234), kind=kOutput, calls=%fused_computation.1.clone.1 | convolution fusion | flops 272628736 | bytes 9048064 | tf_op jit(solution)/shard_map/while/body/eval_jaxpr/qhcd,kcd->cqhk/dot_general | solution.py:82
  185.7 5.3 %fusion.50 = f32[2,512,1,128]{3,1,0,2:T(8,128)S(1)} fusion(f32[2,2048,512]{2,1,0:T(8,128)} %get-tuple-element.202, f32[2,512]{1,0:T(2,128)S(1)} %bitcast.102, f32[2,512,1,128]{3,1,0,2:T(8,128)S(1)} %get-tuple-element.219, bf16[16384,128]{0,1:T(8,128)(2,1)} %get-tuple-element.235, s32[]{:T(128)S(6)} %select_n.17, ...), kind=kOutput, calls=%fused_computation.7.clone.1 | convolution fusion | flops 543555584 | bytes 9969669 | tf_op jit(solution)/shard_map/while/body/eval_jaxpr/cqhk,kv->cqhv/dot_general | solution.py:94
  191.6 1.4 fusion.49
  195.4 4.5 %bitcast_reduce_fusion.2 = (f32[2,512]{1,0:T(2,128)S(1)}, f32[2,2048,512]{2,1,0:T(8,128)}) fusion(bf16[2048,2,64]{0,2,1:T(8,128)(2,1)S(1)} %bitcast.99, bf16[512,1,2,64]{0,3,2,1:T(8,128)(2,1)S(1)} %get-tuple-element.234), kind=kOutput, calls=%fused_computation.1.clone.1 | convolution fusion | flops 272628736 | bytes 9048064 | tf_op jit(solution)/shard_map/while/body/eval_jaxpr/qhcd,kcd->cqhk/dot_general | solution.py:82
  199.9 5.3 %fusion.50 = f32[2,512,1,128]{3,1,0,2:T(8,128)S(1)} fusion(f32[2,2048,512]{2,1,0:T(8,128)} %get-tuple-element.202, f32[2,512]{1,0:T(2,128)S(1)} %bitcast.102, f32[2,512,1,128]{3,1,0,2:T(8,128)S(1)} %get-tuple-element.219, bf16[16384,128]{0,1:T(8,128)(2,1)} %get-tuple-element.235, s32[]{:T(128)S(6)} %select_n.17, ...), kind=kOutput, calls=%fused_computation.7.clone.1 | convolution fusion | flops 543555584 | bytes 9969669 | tf_op jit(solution)/shard_map/while/body/eval_jaxpr/cqhk,kv->cqhv/dot_general | solution.py:94
  205.8 1.4 fusion.49
  209.6 4.5 %bitcast_reduce_fusion.2 = (f32[2,512]{1,0:T(2,128)S(1)}, f32[2,2048,512]{2,1,0:T(8,128)}) fusion(bf16[2048,2,64]{0,2,1:T(8,128)(2,1)S(1)} %bitcast.99, bf16[512,1,2,64]{0,3,2,1:T(8,128)(2,1)S(1)} %get-tuple-element.234), kind=kOutput, calls=%fused_computation.1.clone.1 | convolution fusion | flops 272628736 | bytes 9048064 | tf_op jit(solution)/shard_map/while/body/eval_jaxpr/qhcd,kcd->cqhk/dot_general | solution.py:82
  214.1 5.3 %fusion.50 = f32[2,512,1,128]{3,1,0,2:T(8,128)S(1)} fusion(f32[2,2048,512]{2,1,0:T(8,128)} %get-tuple-element.202, f32[2,512]{1,0:T(2,128)S(1)} %bitcast.102, f32[2,512,1,128]{3,1,0,2:T(8,128)S(1)} %get-tuple-element.219, bf16[16384,128]{0,1:T(8,128)(2,1)} %get-tuple-element.235, s32[]{:T(128)S(6)} %select_n.17, ...), kind=kOutput, calls=%fused_computation.7.clone.1 | convolution fusion | flops 543555584 | bytes 9969669 | tf_op jit(solution)/shard_map/while/body/eval_jaxpr/cqhk,kv->cqhv/dot_general | solution.py:94
  220.0 1.4 fusion.49
  223.8 4.5 %bitcast_reduce_fusion.2 = (f32[2,512]{1,0:T(2,128)S(1)}, f32[2,2048,512]{2,1,0:T(8,128)}) fusion(bf16[2048,2,64]{0,2,1:T(8,128)(2,1)S(1)} %bitcast.99, bf16[512,1,2,64]{0,3,2,1:T(8,128)(2,1)S(1)} %get-tuple-element.234), kind=kOutput, calls=%fused_computation.1.clone.1 | convolution fusion | flops 272628736 | bytes 9048064 | tf_op jit(solution)/shard_map/while/body/eval_jaxpr/qhcd,kcd->cqhk/dot_general | solution.py:82
  228.3 5.3 %fusion.50 = f32[2,512,1,128]{3,1,0,2:T(8,128)S(1)} fusion(f32[2,2048,512]{2,1,0:T(8,128)} %get-tuple-element.202, f32[2,512]{1,0:T(2,128)S(1)} %bitcast.102, f32[2,512,1,128]{3,1,0,2:T(8,128)S(1)} %get-tuple-element.219, bf16[16384,128]{0,1:T(8,128)(2,1)} %get-tuple-element.235, s32[]{:T(128)S(6)} %select_n.17, ...), kind=kOutput, calls=%fused_computation.7.clone.1 | convolution fusion | flops 543555584 | bytes 9969669 | tf_op jit(solution)/shard_map/while/body/eval_jaxpr/cqhk,kv->cqhv/dot_general | solution.py:94
  234.2 1.4 fusion.49
  238.0 4.5 %bitcast_reduce_fusion.2 = (f32[2,512]{1,0:T(2,128)S(1)}, f32[2,2048,512]{2,1,0:T(8,128)}) fusion(bf16[2048,2,64]{0,2,1:T(8,128)(2,1)S(1)} %bitcast.99, bf16[512,1,2,64]{0,3,2,1:T(8,128)(2,1)S(1)} %get-tuple-element.234), kind=kOutput, calls=%fused_computation.1.clone.1 | convolution fusion | flops 272628736 | bytes 9048064 | tf_op jit(solution)/shard_map/while/body/eval_jaxpr/qhcd,kcd->cqhk/dot_general | solution.py:82
  242.5 5.3 %fusion.50 = f32[2,512,1,128]{3,1,0,2:T(8,128)S(1)} fusion(f32[2,2048,512]{2,1,0:T(8,128)} %get-tuple-element.202, f32[2,512]{1,0:T(2,128)S(1)} %bitcast.102, f32[2,512,1,128]{3,1,0,2:T(8,128)S(1)} %get-tuple-element.219, bf16[16384,128]{0,1:T(8,128)(2,1)} %get-tuple-element.235, s32[]{:T(128)S(6)} %select_n.17, ...), kind=kOutput, calls=%fused_computation.7.clone.1 | convolution fusion | flops 543555584 | bytes 9969669 | tf_op jit(solution)/shard_map/while/body/eval_jaxpr/cqhk,kv->cqhv/dot_general | solution.py:94
  248.4 1.4 fusion.49
  252.2 4.5 %bitcast_reduce_fusion.2 = (f32[2,512]{1,0:T(2,128)S(1)}, f32[2,2048,512]{2,1,0:T(8,128)}) fusion(bf16[2048,2,64]{0,2,1:T(8,128)(2,1)S(1)} %bitcast.99, bf16[512,1,2,64]{0,3,2,1:T(8,128)(2,1)S(1)} %get-tuple-element.234), kind=kOutput, calls=%fused_computation.1.clone.1 | convolution fusion | flops 272628736 | bytes 9048064 | tf_op jit(solution)/shard_map/while/body/eval_jaxpr/qhcd,kcd->cqhk/dot_general | solution.py:82
  256.7 5.3 %fusion.50 = f32[2,512,1,128]{3,1,0,2:T(8,128)S(1)} fusion(f32[2,2048,512]{2,1,0:T(8,128)} %get-tuple-element.202, f32[2,512]{1,0:T(2,128)S(1)} %bitcast.102, f32[2,512,1,128]{3,1,0,2:T(8,128)S(1)} %get-tuple-element.219, bf16[16384,128]{0,1:T(8,128)(2,1)} %get-tuple-element.235, s32[]{:T(128)S(6)} %select_n.17, ...), kind=kOutput, calls=%fused_computation.7.clone.1 | convolution fusion | flops 543555584 | bytes 9969669 | tf_op jit(solution)/shard_map/while/body/eval_jaxpr/cqhk,kv->cqhv/dot_general | solution.py:94
  264.9 13.2 %all_to_all.21 = bf16[8,64,128]{2,1,0:T(8,128)(2,1)S(1)} all-to-all(bf16[8,64,128]{2,1,0:T(8,128)(2,1)S(1)} %multiply_convert_fusion), channel_id=1, replica_groups=mesh['sp'=32,'tp'=8] {'tp'}, dimensions={0} | all-to-all | bytes 262144 | tf_op jit(solution)/shard_map/all_to_all | solution.py:125
  278.1 3.7 %convolution_convert_fusion = bf16[64,2048]{1,0:T(8,128)(2,1)} fusion(bf16[1024,2048]{1,0:T(8,128)(2,1)} %param.13, bf16[8,64,128]{2,1,0:T(8,128)(2,1)S(1)} %all_to_all.21), kind=kOutput, calls=%fused_computation.22 | convolution fusion | flops 268566528 | bytes 4587520 | tf_op jit(solution)/shard_map/dot_general | solution.py:126
  (84 shorter events, 23.5 us)
Async XLA Ops:
  9.1 32.9 %all-to-all-start = ((bf16[8,64,2048]{2,1,0:T(8,128)(2,1)}), bf16[8,64,2048]{2,1,0:T(8,128)(2,1)S(1)}, u32[]{:S(2)}, u32[]{:S(2)}) async-start(bf16[8,64,2048]{2,1,0:T(8,128)(2,1)} %broadcast_in_dim.11), calls=%async_computation | async-start | bytes 4194304 | tf_op jit(solution)/shard_map/all_to_all | solution.py:22
  15.8 128.8 %all-gather.2.cloned.1.call-start = ((), (), s32[]{:S(2)}) async-start(), calls=%async_computation.2 | async-start | bytes 8650752 | tf_op jit(solution)/shard_map/all_gather | solution.py:35
  150.4 114.2 %copy-start.1 = (f32[128]{0:T(128)S(1)}, f32[128]{0:T(128)}, u32[]{:S(2)}) copy-start(f32[128]{0:T(128)} %param.14) | copy-start | bytes 1540
  157.3 5.9 %copy-start = (f32[2,2048,512]{2,1,0:T(8,128)S(1)}, f32[2,2048,512]{2,1,0:T(8,128)}, u32[]{:S(2)}) copy-start(f32[2,2048,512]{2,1,0:T(8,128)} %get-tuple-element.202) | copy-start | bytes 25165828 | tf_op jit(solution)/shard_map/while
  171.5 5.9 %copy-start = (f32[2,2048,512]{2,1,0:T(8,128)S(1)}, f32[2,2048,512]{2,1,0:T(8,128)}, u32[]{:S(2)}) copy-start(f32[2,2048,512]{2,1,0:T(8,128)} %get-tuple-element.202) | copy-start | bytes 25165828 | tf_op jit(solution)/shard_map/while
  185.7 5.9 %copy-start = (f32[2,2048,512]{2,1,0:T(8,128)S(1)}, f32[2,2048,512]{2,1,0:T(8,128)}, u32[]{:S(2)}) copy-start(f32[2,2048,512]{2,1,0:T(8,128)} %get-tuple-element.202) | copy-start | bytes 25165828 | tf_op jit(solution)/shard_map/while
  199.9 5.9 %copy-start = (f32[2,2048,512]{2,1,0:T(8,128)S(1)}, f32[2,2048,512]{2,1,0:T(8,128)}, u32[]{:S(2)}) copy-start(f32[2,2048,512]{2,1,0:T(8,128)} %get-tuple-element.202) | copy-start | bytes 25165828 | tf_op jit(solution)/shard_map/while
  214.1 5.9 %copy-start = (f32[2,2048,512]{2,1,0:T(8,128)S(1)}, f32[2,2048,512]{2,1,0:T(8,128)}, u32[]{:S(2)}) copy-start(f32[2,2048,512]{2,1,0:T(8,128)} %get-tuple-element.202) | copy-start | bytes 25165828 | tf_op jit(solution)/shard_map/while
  228.3 5.9 %copy-start = (f32[2,2048,512]{2,1,0:T(8,128)S(1)}, f32[2,2048,512]{2,1,0:T(8,128)}, u32[]{:S(2)}) copy-start(f32[2,2048,512]{2,1,0:T(8,128)} %get-tuple-element.202) | copy-start | bytes 25165828 | tf_op jit(solution)/shard_map/while
  242.5 5.9 %copy-start = (f32[2,2048,512]{2,1,0:T(8,128)S(1)}, f32[2,2048,512]{2,1,0:T(8,128)}, u32[]{:S(2)}) copy-start(f32[2,2048,512]{2,1,0:T(8,128)} %get-tuple-element.202) | copy-start | bytes 25165828 | tf_op jit(solution)/shard_map/while
  256.7 5.9 %copy-start = (f32[2,2048,512]{2,1,0:T(8,128)S(1)}, f32[2,2048,512]{2,1,0:T(8,128)}, u32[]{:S(2)}) copy-start(f32[2,2048,512]{2,1,0:T(8,128)} %get-tuple-element.202) | copy-start | bytes 25165828 | tf_op jit(solution)/shard_map/while
Sparse Core Ops, SparseCore 0:
  45.1 99.4 all-gather.1
where the time goes:
time: 289 us
  waiting for transfers between devices  124 us (43%)
  matrix products  84.1 us (29%)
  local copies, waits for them, and re-layouts  28.4 us (10%)
  between operations  14.2 us (5%)
  blocking collectives  13.2 us (5%)
  other arithmetic  13 us (4%)
  starting transfers between devices  6.71 us (2%)
  loops' own time  5.6 us (2%)
    all_gather x1, waiting for transfers between devices, sent_together(): lax.all_gather(both, axis, axis=dim, tiled=True)  98.9 us
    dot_general x8, matrix products, update(): jnp.einsum('cqhk,kv->cqhv', weights.astype(jnp.bfloat16), value_block, pr...  42.1 us
    dot_general x8, matrix products, update(): jnp.einsum('qhcd,kcd->cqhk', queries, key_block.reshape(key_block.shape[0...  36.2 us
    all_to_all x1, waiting for transfers between devices, copy_for_each(): lax.all_to_all(jnp.broadcast_to(x[None], (count, *x.shape)), axis, 0, 0,...  24.6 us
    all_to_all x1, blocking collectives, local(): lax.all_to_all(normed, 'tp', split_axis=0, concat_axis=1, tiled=True)  13.2 us
    reduce_sum x8, other arithmetic, update(): running_sum = shrink * running_sum + jnp.sum(weights, axis=-1)  11 us
    dynamic_slice x8, local copies, waits for them, and re-layouts, one_span(): lax.dynamic_slice_in_dim(key_piece, span_index * fold_span, fold_span, 0)  8.65 us
    all_to_all x1, starting transfers between devices, copy_for_each(): lax.all_to_all(jnp.broadcast_to(x[None], (count, *x.shape)), axis, 0, 0,...  6.7 us
  transfers between devices with their start and end apart: 2, of which 2 were waited for; matrix products, arithmetic and copies ran while one was open for 1% of the time, Pallas kernels for 0%

commit v1 on v0

--- a/solution.py
+++ b/solution.py
@@ -51,6 +51,19 @@
 
 
 def local(tokens, query_weight, key_weight, value_weight, out_weight, head_gain, lambdas):
+
+    def map_ranges(content):
+        v_next = jnp.concatenate(
+            lax.all_to_all(
+                jnp.stack(jnp.split(content, lax.axis_size("tp"), axis=0), axis=0),
+                split_axis=0,
+                concat_axis=0,
+                axis_name="tp",
+            ),
+            axis=1,
+        )
+        return v_next
+
     heads_dev = query_weight.shape[1] // (2 * DH)
     kv_heads = key_weight.shape[1] // (2 * DH)
     group_size = H // kv_heads
@@ -122,7 +135,7 @@
     mean_square = jnp.mean(attended * attended, axis=-1, keepdims=True)
     normed = (attended * lax.rsqrt(mean_square + epsilon) * head_gain).astype(jnp.bfloat16)
     normed = normed.reshape(seq_rows, heads_dev * DV)
-    regrouped = lax.all_to_all(normed, "tp", split_axis=0, concat_axis=1, tiled=True)
+    regrouped = map_ranges(normed)
     return jnp.dot(regrouped, out_weight, preferred_element_type=jnp.float32).astype(jnp.bfloat16)
 
 

time: 289 us -> 289 us (level)
  no operation moved by 1% of the time
where the time goes in v1:
time: 289 us; the launch traced here: 288 us
  waiting for transfers between devices  124 us (43%)
  matrix products  84.1 us (29%)
  local copies, waits for them, and re-layouts  28.2 us (10%)
  between operations  14.2 us (5%)
  blocking collectives  13.2 us (5%)
  other arithmetic  12.8 us (4%)
  starting transfers between devices  6.71 us (2%)
  loops' own time  5.6 us (2%)
    all_gather x1, waiting for transfers between devices, sent_together(): lax.all_gather(both, axis, axis=dim, tiled=True)  98.9 us
    dot_general x8, matrix products, update(): jnp.einsum('cqhk,kv->cqhv', weights.astype(jnp.bfloat16), value_block, pr...  42.1 us
    dot_general x8, matrix products, update(): jnp.einsum('qhcd,kcd->cqhk', queries, key_block.reshape(key_block.shape[0...  36.2 us
    all_to_all x1, waiting for transfers between devices, copy_for_each(): lax.all_to_all(jnp.broadcast_to(x[None], (count, *x.shape)), axis, 0, 0,...  24.6 us
    all_to_all x1, blocking collectives, map_ranges(): lax.all_to_all(jnp.stack(jnp.split(content, lax.axis_size('tp'), axis=0),...  13.2 us
    reduce_sum x8, other arithmetic, update(): running_sum = shrink * running_sum + jnp.sum(weights, axis=-1)  11 us
    dynamic_slice x8, local copies, waits for them, and re-layouts, one_span(): lax.dynamic_slice_in_dim(key_piece, span_index * fold_span, fold_span, 0)  8.65 us
    all_to_all x1, starting transfers between devices, copy_for_each(): lax.all_to_all(jnp.broadcast_to(x[None], (count, *x.shape)), axis, 0, 0,...  6.7 us
  transfers between devices with their start and end apart: 2, of which 2 were waited for; matrix products, arithmetic and copies ran while one was open for 1% of the time, Pallas kernels for 0%

profile of v1, /device:TPU:1, one launch (start us, length us, event | category | flops | bytes accessed | tf_op | source)
XLA Modules:
  0.0 288.4 jit_solution(2157014576865928422)
XLA Ops:
  6.5 2.5 broadcast_in_dim.11
  9.1 6.7 %all-to-all-start = ((bf16[8,64,2048]{2,1,0:T(8,128)(2,1)}), bf16[8,64,2048]{2,1,0:T(8,128)(2,1)S(1)}, u32[]{:S(2)}, u32[]{:S(2)}) async-start(bf16[8,64,2048]{2,1,0:T(8,128)(2,1)} %broadcast_in_dim.11), calls=%async_computation | async-start | bytes 4194304 | tf_op jit(solution)/shard_map/all_to_all | solution.py:22
  17.4 24.6 %all-to-all-done = bf16[8,64,2048]{2,1,0:T(8,128)(2,1)S(1)} async-done(((bf16[8,64,2048]{2,1,0:T(8,128)(2,1)}), bf16[8,64,2048]{2,1,0:T(8,128)(2,1)S(1)}, u32[]{:S(2)}, u32[]{:S(2)}) %all-to-all-start) | async-done | bytes 2097184 | tf_op jit(solution)/shard_map/all_to_all | solution.py:22
  42.0 2.1 fusion.24
  45.7 98.9 %all-gather.2.cloned.1.call-done = bf16[16384,256]{0,1:T(8,128)(2,1)} async-done(((bf16[512,256]{0,1:T(8,128)(2,1)}), bf16[16384,256]{0,1:T(8,128)(2,1)}) %all-gather.2.cloned.1.call-update) | async-done | bytes 8388624 | tf_op jit(solution)/shard_map/all_gather | solution.py:35
  144.6 5.8 %fusion.33 = (bf16[16384,128]{0,1:T(8,128)(2,1)}, bf16[16384,128]{0,1:T(8,128)(2,1)}) fusion(bf16[16384,256]{0,1:T(8,128)(2,1)} %all-gather.2.cloned.1.call-done), kind=kLoop, calls=%fused_computation.70 | loop fusion | bytes 16777216 | tf_op jit(solution)/shard_map/split | solution.py:35
  150.4 113.6 %while.15 = (s32[]{:T(128)}, f32[2,512,1]{1,0,2:T(2,128)S(1)}, f32[2,512,1]{1,0,2:T(2,128)S(1)}, f32[2,512,1,128]{3,1,0,2:T(8,128)S(1)}, s32[8]{0:T(128)S(1)}, /...) while((s32[]{:T(128)}, f32[2,512,1]{1,0,2:T(2,128)S(1)}, ...), condition=%wide.region_3.4_spmd.clone, body=%wide.region_0.3_spmd.clone.sunk | while | flops 822482944 | bytes 62062812 | solution.py:128
  152.8 4.5 %bitcast_reduce_fusion.2 = (f32[2,512]{1,0:T(2,128)S(1)}, f32[2,2048,512]{2,1,0:T(8,128)}) fusion(bf16[2048,2,64]{0,2,1:T(8,128)(2,1)S(1)} %bitcast.127, bf16[512,1,2,64]{0,3,2,1:T(8,128)(2,1)S(1)} %get-tuple-element.216), kind=kOutput, calls=%fused_computation.1.clone.1 | convolution fusion | flops 272628736 | bytes 9048064 | tf_op jit(solution)/shard_map/while/body/eval_jaxpr/qhcd,kcd->cqhk/dot_general | solution.py:95
  157.3 5.3 %fusion.51 = f32[2,512,1,128]{3,1,0,2:T(8,128)S(1)} fusion(f32[2,2048,512]{2,1,0:T(8,128)} %get-tuple-element.184, f32[2,512]{1,0:T(2,128)S(1)} %bitcast.129, f32[2,512,1,128]{3,1,0,2:T(8,128)S(1)} %get-tuple-element.201, bf16[16384,128]{0,1:T(8,128)(2,1)} %get-tuple-element.217, s32[]{:T(128)S(6)} %select_n.17, ...), kind=kOutput, calls=%fused_computation.7.clone.1 | convolution fusion | flops 543555584 | bytes 9969669 | tf_op jit(solution)/shard_map/while/body/eval_jaxpr/cqhk,kv->cqhv/dot_general | solution.py:107
  163.2 1.4 fusion.50
  167.0 4.5 %bitcast_reduce_fusion.2 = (f32[2,512]{1,0:T(2,128)S(1)}, f32[2,2048,512]{2,1,0:T(8,128)}) fusion(bf16[2048,2,64]{0,2,1:T(8,128)(2,1)S(1)} %bitcast.127, bf16[512,1,2,64]{0,3,2,1:T(8,128)(2,1)S(1)} %get-tuple-element.216), kind=kOutput, calls=%fused_computation.1.clone.1 | convolution fusion | flops 272628736 | bytes 9048064 | tf_op jit(solution)/shard_map/while/body/eval_jaxpr/qhcd,kcd->cqhk/dot_general | solution.py:95
  171.5 5.3 %fusion.51 = f32[2,512,1,128]{3,1,0,2:T(8,128)S(1)} fusion(f32[2,2048,512]{2,1,0:T(8,128)} %get-tuple-element.184, f32[2,512]{1,0:T(2,128)S(1)} %bitcast.129, f32[2,512,1,128]{3,1,0,2:T(8,128)S(1)} %get-tuple-element.201, bf16[16384,128]{0,1:T(8,128)(2,1)} %get-tuple-element.217, s32[]{:T(128)S(6)} %select_n.17, ...), kind=kOutput, calls=%fused_computation.7.clone.1 | convolution fusion | flops 543555584 | bytes 9969669 | tf_op jit(solution)/shard_map/while/body/eval_jaxpr/cqhk,kv->cqhv/dot_general | solution.py:107
  177.4 1.4 fusion.50
  181.2 4.5 %bitcast_reduce_fusion.2 = (f32[2,512]{1,0:T(2,128)S(1)}, f32[2,2048,512]{2,1,0:T(8,128)}) fusion(bf16[2048,2,64]{0,2,1:T(8,128)(2,1)S(1)} %bitcast.127, bf16[512,1,2,64]{0,3,2,1:T(8,128)(2,1)S(1)} %get-tuple-element.216), kind=kOutput, calls=%fused_computation.1.clone.1 | convolution fusion | flops 272628736 | bytes 9048064 | tf_op jit(solution)/shard_map/while/body/eval_jaxpr/qhcd,kcd->cqhk/dot_general | solution.py:95
  185.7 5.3 %fusion.51 = f32[2,512,1,128]{3,1,0,2:T(8,128)S(1)} fusion(f32[2,2048,512]{2,1,0:T(8,128)} %get-tuple-element.184, f32[2,512]{1,0:T(2,128)S(1)} %bitcast.129, f32[2,512,1,128]{3,1,0,2:T(8,128)S(1)} %get-tuple-element.201, bf16[16384,128]{0,1:T(8,128)(2,1)} %get-tuple-element.217, s32[]{:T(128)S(6)} %select_n.17, ...), kind=kOutput, calls=%fused_computation.7.clone.1 | convolution fusion | flops 543555584 | bytes 9969669 | tf_op jit(solution)/shard_map/while/body/eval_jaxpr/cqhk,kv->cqhv/dot_general | solution.py:107
  191.6 1.4 fusion.50
  195.4 4.5 %bitcast_reduce_fusion.2 = (f32[2,512]{1,0:T(2,128)S(1)}, f32[2,2048,512]{2,1,0:T(8,128)}) fusion(bf16[2048,2,64]{0,2,1:T(8,128)(2,1)S(1)} %bitcast.127, bf16[512,1,2,64]{0,3,2,1:T(8,128)(2,1)S(1)} %get-tuple-element.216), kind=kOutput, calls=%fused_computation.1.clone.1 | convolution fusion | flops 272628736 | bytes 9048064 | tf_op jit(solution)/shard_map/while/body/eval_jaxpr/qhcd,kcd->cqhk/dot_general | solution.py:95
  199.9 5.3 %fusion.51 = f32[2,512,1,128]{3,1,0,2:T(8,128)S(1)} fusion(f32[2,2048,512]{2,1,0:T(8,128)} %get-tuple-element.184, f32[2,512]{1,0:T(2,128)S(1)} %bitcast.129, f32[2,512,1,128]{3,1,0,2:T(8,128)S(1)} %get-tuple-element.201, bf16[16384,128]{0,1:T(8,128)(2,1)} %get-tuple-element.217, s32[]{:T(128)S(6)} %select_n.17, ...), kind=kOutput, calls=%fused_computation.7.clone.1 | convolution fusion | flops 543555584 | bytes 9969669 | tf_op jit(solution)/shard_map/while/body/eval_jaxpr/cqhk,kv->cqhv/dot_general | solution.py:107
  205.8 1.4 fusion.50
  209.6 4.5 %bitcast_reduce_fusion.2 = (f32[2,512]{1,0:T(2,128)S(1)}, f32[2,2048,512]{2,1,0:T(8,128)}) fusion(bf16[2048,2,64]{0,2,1:T(8,128)(2,1)S(1)} %bitcast.127, bf16[512,1,2,64]{0,3,2,1:T(8,128)(2,1)S(1)} %get-tuple-element.216), kind=kOutput, calls=%fused_computation.1.clone.1 | convolution fusion | flops 272628736 | bytes 9048064 | tf_op jit(solution)/shard_map/while/body/eval_jaxpr/qhcd,kcd->cqhk/dot_general | solution.py:95
  214.1 5.3 %fusion.51 = f32[2,512,1,128]{3,1,0,2:T(8,128)S(1)} fusion(f32[2,2048,512]{2,1,0:T(8,128)} %get-tuple-element.184, f32[2,512]{1,0:T(2,128)S(1)} %bitcast.129, f32[2,512,1,128]{3,1,0,2:T(8,128)S(1)} %get-tuple-element.201, bf16[16384,128]{0,1:T(8,128)(2,1)} %get-tuple-element.217, s32[]{:T(128)S(6)} %select_n.17, ...), kind=kOutput, calls=%fused_computation.7.clone.1 | convolution fusion | flops 543555584 | bytes 9969669 | tf_op jit(solution)/shard_map/while/body/eval_jaxpr/cqhk,kv->cqhv/dot_general | solution.py:107
  220.1 1.4 fusion.50
  223.8 4.5 %bitcast_reduce_fusion.2 = (f32[2,512]{1,0:T(2,128)S(1)}, f32[2,2048,512]{2,1,0:T(8,128)}) fusion(bf16[2048,2,64]{0,2,1:T(8,128)(2,1)S(1)} %bitcast.127, bf16[512,1,2,64]{0,3,2,1:T(8,128)(2,1)S(1)} %get-tuple-element.216), kind=kOutput, calls=%fused_computation.1.clone.1 | convolution fusion | flops 272628736 | bytes 9048064 | tf_op jit(solution)/shard_map/while/body/eval_jaxpr/qhcd,kcd->cqhk/dot_general | solution.py:95
  228.4 5.3 %fusion.51 = f32[2,512,1,128]{3,1,0,2:T(8,128)S(1)} fusion(f32[2,2048,512]{2,1,0:T(8,128)} %get-tuple-element.184, f32[2,512]{1,0:T(2,128)S(1)} %bitcast.129, f32[2,512,1,128]{3,1,0,2:T(8,128)S(1)} %get-tuple-element.201, bf16[16384,128]{0,1:T(8,128)(2,1)} %get-tuple-element.217, s32[]{:T(128)S(6)} %select_n.17, ...), kind=kOutput, calls=%fused_computation.7.clone.1 | convolution fusion | flops 543555584 | bytes 9969669 | tf_op jit(solution)/shard_map/while/body/eval_jaxpr/cqhk,kv->cqhv/dot_general | solution.py:107
  234.3 1.4 fusion.50
  238.0 4.5 %bitcast_reduce_fusion.2 = (f32[2,512]{1,0:T(2,128)S(1)}, f32[2,2048,512]{2,1,0:T(8,128)}) fusion(bf16[2048,2,64]{0,2,1:T(8,128)(2,1)S(1)} %bitcast.127, bf16[512,1,2,64]{0,3,2,1:T(8,128)(2,1)S(1)} %get-tuple-element.216), kind=kOutput, calls=%fused_computation.1.clone.1 | convolution fusion | flops 272628736 | bytes 9048064 | tf_op jit(solution)/shard_map/while/body/eval_jaxpr/qhcd,kcd->cqhk/dot_general | solution.py:95
  242.6 5.3 %fusion.51 = f32[2,512,1,128]{3,1,0,2:T(8,128)S(1)} fusion(f32[2,2048,512]{2,1,0:T(8,128)} %get-tuple-element.184, f32[2,512]{1,0:T(2,128)S(1)} %bitcast.129, f32[2,512,1,128]{3,1,0,2:T(8,128)S(1)} %get-tuple-element.201, bf16[16384,128]{0,1:T(8,128)(2,1)} %get-tuple-element.217, s32[]{:T(128)S(6)} %select_n.17, ...), kind=kOutput, calls=%fused_computation.7.clone.1 | convolution fusion | flops 543555584 | bytes 9969669 | tf_op jit(solution)/shard_map/while/body/eval_jaxpr/cqhk,kv->cqhv/dot_general | solution.py:107
  252.2 4.5 %bitcast_reduce_fusion.2 = (f32[2,512]{1,0:T(2,128)S(1)}, f32[2,2048,512]{2,1,0:T(8,128)}) fusion(bf16[2048,2,64]{0,2,1:T(8,128)(2,1)S(1)} %bitcast.127, bf16[512,1,2,64]{0,3,2,1:T(8,128)(2,1)S(1)} %get-tuple-element.216), kind=kOutput, calls=%fused_computation.1.clone.1 | convolution fusion | flops 272628736 | bytes 9048064 | tf_op jit(solution)/shard_map/while/body/eval_jaxpr/qhcd,kcd->cqhk/dot_general | solution.py:95
  256.8 5.3 %fusion.51 = f32[2,512,1,128]{3,1,0,2:T(8,128)S(1)} fusion(f32[2,2048,512]{2,1,0:T(8,128)} %get-tuple-element.184, f32[2,512]{1,0:T(2,128)S(1)} %bitcast.129, f32[2,512,1,128]{3,1,0,2:T(8,128)S(1)} %get-tuple-element.201, bf16[16384,128]{0,1:T(8,128)(2,1)} %get-tuple-element.217, s32[]{:T(128)S(6)} %select_n.17, ...), kind=kOutput, calls=%fused_computation.7.clone.1 | convolution fusion | flops 543555584 | bytes 9969669 | tf_op jit(solution)/shard_map/while/body/eval_jaxpr/cqhk,kv->cqhv/dot_general | solution.py:107
  262.7 1.4 fusion.50
  264.7 13.2 %all_to_all.10 = bf16[8,64,128]{2,1,0:T(8,128)(2,1)S(1)} all-to-all(bf16[8,64,128]{2,1,0:T(8,128)(2,1)S(1)} %constant_dynamic-update-slice_fusion), channel_id=1, replica_groups=mesh['sp'=32,'tp'=8] {'tp'}, dimensions={0} | all-to-all | bytes 262144 | tf_op jit(solution)/shard_map/all_to_all | solution.py:57
  277.9 3.7 %convolution_convert_fusion = bf16[64,2048]{1,0:T(8,128)(2,1)} fusion(bf16[1024,2048]{1,0:T(8,128)(2,1)} %param.13, bf16[8,64,128]{2,1,0:T(8,128)(2,1)S(1)} %all_to_all.10), kind=kOutput, calls=%fused_computation.22 | convolution fusion | flops 268566528 | bytes 4587520 | tf_op jit(solution)/shard_map/dot_general | solution.py:139
  (88 shorter events, 23.2 us)
Async XLA Ops:
  9.1 32.9 %all-to-all-start = ((bf16[8,64,2048]{2,1,0:T(8,128)(2,1)}), bf16[8,64,2048]{2,1,0:T(8,128)(2,1)S(1)}, u32[]{:S(2)}, u32[]{:S(2)}) async-start(bf16[8,64,2048]{2,1,0:T(8,128)(2,1)} %broadcast_in_dim.11), calls=%async_computation | async-start | bytes 4194304 | tf_op jit(solution)/shard_map/all_to_all | solution.py:22
  15.8 128.8 %all-gather.2.cloned.1.call-start = ((), (), s32[]{:S(2)}) async-start(), calls=%async_computation.2 | async-start | bytes 8650752 | tf_op jit(solution)/shard_map/all_gather | solution.py:35
  150.4 114.0 %copy-start.1 = (f32[128]{0:T(128)S(1)}, f32[128]{0:T(128)}, u32[]{:S(2)}) copy-start(f32[128]{0:T(128)} %param.14) | copy-start | bytes 1540
  157.3 5.9 %copy-start = (f32[2,2048,512]{2,1,0:T(8,128)S(1)}, f32[2,2048,512]{2,1,0:T(8,128)}, u32[]{:S(2)}) copy-start(f32[2,2048,512]{2,1,0:T(8,128)} %get-tuple-element.184) | copy-start | bytes 25165828 | tf_op jit(solution)/shard_map/while
  171.5 5.9 %copy-start = (f32[2,2048,512]{2,1,0:T(8,128)S(1)}, f32[2,2048,512]{2,1,0:T(8,128)}, u32[]{:S(2)}) copy-start(f32[2,2048,512]{2,1,0:T(8,128)} %get-tuple-element.184) | copy-start | bytes 25165828 | tf_op jit(solution)/shard_map/while
  185.7 5.9 %copy-start = (f32[2,2048,512]{2,1,0:T(8,128)S(1)}, f32[2,2048,512]{2,1,0:T(8,128)}, u32[]{:S(2)}) copy-start(f32[2,2048,512]{2,1,0:T(8,128)} %get-tuple-element.184) | copy-start | bytes 25165828 | tf_op jit(solution)/shard_map/while
  199.9 5.9 %copy-start = (f32[2,2048,512]{2,1,0:T(8,128)S(1)}, f32[2,2048,512]{2,1,0:T(8,128)}, u32[]{:S(2)}) copy-start(f32[2,2048,512]{2,1,0:T(8,128)} %get-tuple-element.184) | copy-start | bytes 25165828 | tf_op jit(solution)/shard_map/while
  214.1 5.9 %copy-start = (f32[2,2048,512]{2,1,0:T(8,128)S(1)}, f32[2,2048,512]{2,1,0:T(8,128)}, u32[]{:S(2)}) copy-start(f32[2,2048,512]{2,1,0:T(8,128)} %get-tuple-element.184) | copy-start | bytes 25165828 | tf_op jit(solution)/shard_map/while
  228.3 5.9 %copy-start = (f32[2,2048,512]{2,1,0:T(8,128)S(1)}, f32[2,2048,512]{2,1,0:T(8,128)}, u32[]{:S(2)}) copy-start(f32[2,2048,512]{2,1,0:T(8,128)} %get-tuple-element.184) | copy-start | bytes 25165828 | tf_op jit(solution)/shard_map/while
  242.5 5.9 %copy-start = (f32[2,2048,512]{2,1,0:T(8,128)S(1)}, f32[2,2048,512]{2,1,0:T(8,128)}, u32[]{:S(2)}) copy-start(f32[2,2048,512]{2,1,0:T(8,128)} %get-tuple-element.184) | copy-start | bytes 25165828 | tf_op jit(solution)/shard_map/while
  256.8 5.9 %copy-start = (f32[2,2048,512]{2,1,0:T(8,128)S(1)}, f32[2,2048,512]{2,1,0:T(8,128)}, u32[]{:S(2)}) copy-start(f32[2,2048,512]{2,1,0:T(8,128)} %get-tuple-element.184) | copy-start | bytes 25165828 | tf_op jit(solution)/shard_map/while
Sparse Core Ops, SparseCore 0:
  45.1 99.4 all-gather.1
